TPU v7x, 512 devices: a whole 4x4x16 slice. The times are simulated.
512 devices in a mesh: sp: 64 (over z, y), tp: 8 (over x, core).
Axes of the slice: x: 4, y: 4, z: 16, core: 2. Of those that a mesh axis runs over, the one named last changes fastest.
Arguments:
- layer_input_sequence: bfloat16 [24576, 2048], P('sp', 'tp'), may hold values from -6 to 6
- probe_projection_matrix: bfloat16 [2048, 1024], P(None, 'tp'), may hold values from -0.125 to 0.125
- address_projection_matrix: bfloat16 [2048, 1024], P(None, 'tp'), may hold values from -0.125 to 0.125
- content_projection_matrix: bfloat16 [2048, 1024], P(None, 'tp'), may hold values from -2 to 2
- result_valve_matrix: bfloat16 [2048, 1024], P(None, 'tp'), may hold values from -0.125 to 0.125
- shrink_strength_matrix: bfloat16 [2, 2048, 8], replicated, may hold values from -0.125 to 0.125
- causal_filter_coefficients: bfloat16 [3, 4, 1024], P(None, None, 'tp'), may hold values from -3 to 3
- channel_group_fading_speed: float32 [8], replicated, may hold values from 0 to 0.06, as said below
- summed_shrink_logs: float32 [24576, 8], P('sp', 'tp'), may hold values from -0.7 to 0, as said below
- result_scaling_vector: bfloat16 [128], replicated, may hold values from 0.099609375 to 1.8984375
- generated_probe_vector: bfloat16 [64, 8, 128], P('sp', 'tp'), may hold values from -6 to 6
Outputs:
- mixed: bfloat16 [24576, 1024], P('sp', 'tp')
- cache: bfloat16 [8, 128, 128], P('tp')
- new_read: float32 [64, 8, 128], P('sp', 'tp')
Inputs may be any that keep to these rules, and one draw needn't show every extreme that they name: `channel_group_fading_speed`: positive rates of each head. `summed_shrink_logs`: zero at all but a few positions of each head.
All inputs are finite; a program needn't handle non-finite values.
Results may differ from a plain program's by a relative error of at most 0.0095.
Values may be sent and summed in bfloat16 or wider, within the bound.
A program may use at most 64 MiB of HBM per device.

v0:
```python
import math

import jax
import jax.numpy as jnp
from jax import lax
from jax.sharding import PartitionSpec as P

DK = 128
BLK = 64
CONV = 4


EPS = 1e-06
HIGH = lax.Precision.HIGHEST


def sent_to_all(shard, axis):
    count = lax.axis_size(axis)
    return lax.all_to_all(
        jnp.broadcast_to(shard[None], (count, *shard.shape)), axis, 0, 0, tiled=True
    )


def in_order(pieces, dim):
    dims = list(pieces.shape[1:])
    dims[dim] *= pieces.shape[0]
    return jnp.moveaxis(pieces, 0, dim).reshape(dims)


def gathered_copies(shard, axis, dim):
    pieces = sent_to_all(shard, axis)
    return in_order(pieces, dim)


def shifted(block, axis, distance):
    devices = range(lax.axis_size(axis))
    route = [(i - distance, i) for i in devices if i - distance in devices]
    return lax.ppermute(block, axis, route)


def silu(value):
    return value * jax.nn.sigmoid(value)


def l2_unit(value):
    return value * lax.rsqrt(jnp.sum(value * value, axis=-1, keepdims=True) + EPS)


def block_terms(query, keys, values, fading_exponent, beta):
    heads, length, width = keys.shape
    count = length // BLK

    def split(array):
        return array.reshape((heads, count, BLK) + array.shape[2:])

    query, keys, values, fading_exponent, beta = (
        split(a) for a in (query, keys, values, fading_exponent, beta)
    )
    summed = jnp.cumsum(fading_exponent, axis=-1)
    places = jnp.arange(BLK)
    inclusive = places[:, None] >= places[None, :]
    strict = places[:, None] > places[None, :]
    decay = jnp.exp(jnp.where(inclusive, summed[..., :, None] - summed[..., None, :], -1e30))
    k_beta = keys * beta[..., None]
    a_mat = jnp.where(
        strict, jnp.einsum("hncd,hnsd->hncs", k_beta, keys, precision=HIGH) * decay, 0.0
    )
    eye = jnp.eye(BLK, dtype=jnp.float32)
    t_mat = lax.linalg.triangular_solve(
        eye + a_mat,
        jnp.broadcast_to(eye, a_mat.shape),
        left_side=True,
        lower=True,
        unit_diagonal=True,
    )
    u_part = jnp.einsum("hncs,hnsd->hncd", t_mat, values * beta[..., None], precision=HIGH)
    w_part = jnp.einsum(
        "hncs,hnsd->hncd", t_mat, k_beta * jnp.exp(summed)[..., None], precision=HIGH
    )
    attend = jnp.where(
        inclusive, jnp.einsum("hncd,hnsd->hncs", query, keys, precision=HIGH) * decay, 0.0
    )
    q_dec = query * jnp.exp(summed)[..., None]
    k_dec = keys * jnp.exp(summed[..., -1:] - summed)[..., None]
    g_last = jnp.exp(summed[..., -1])
    return (u_part, w_part, q_dec, k_dec, attend, g_last)


def matmul_heads(left, right):
    return jnp.einsum("hij,hjk->hik", left, right, precision=HIGH)


def on_device(
    layer_input_sequence,
    probe_projection_matrix,
    address_projection_matrix,
    content_projection_matrix,
    result_valve_matrix,
    shrink_strength_matrix,
    causal_filter_coefficients,
    channel_group_fading_speed,
    summed_shrink_logs,
    result_scaling_vector,
    generated_probe_vector,
):
    tok_rows = layer_input_sequence.shape[0]
    local_width = probe_projection_matrix.shape[1]
    head_count = local_width // DK
    prompt_length = tok_rows * lax.axis_size("sp")
    piece = gathered_copies(layer_input_sequence, "tp", 1)
    columns = [
        m
        for m in (
            probe_projection_matrix,
            address_projection_matrix,
            content_projection_matrix,
            result_valve_matrix,
        )
    ]
    projected = jnp.stack([jnp.dot(piece, c, preferred_element_type=jnp.float32) for c in columns])
    rate_terms = jnp.einsum(
        "sd,rdh->srh", piece, shrink_strength_matrix, preferred_element_type=jnp.float32
    )
    projected, rate_terms = (projected, rate_terms)
    raw = projected.astype(jnp.bfloat16)
    rim = shifted(raw[:3, tok_rows - (CONV - 1) :], "sp", 1)
    extended = jnp.concatenate([rim, raw[:3]], axis=1).astype(jnp.float32)
    taps = causal_filter_coefficients.astype(jnp.float32)
    summed_taps = jnp.zeros((3, tok_rows, local_width), jnp.float32)
    for lag in range(CONV):
        summed_taps = summed_taps + taps[:, lag, None, :] * extended[:, lag : lag + tok_rows]
    convolved = silu(summed_taps)
    query = l2_unit(convolved[0].reshape(tok_rows, head_count, DK)) * DK ** (-0.5)
    keys = l2_unit(convolved[1].reshape(tok_rows, head_count, DK))
    values = convolved[2].reshape(tok_rows, head_count, DK)
    first_head = lax.axis_index("tp") * head_count
    diagonal_speed_entries = lax.dynamic_slice_in_dim(rate_terms, first_head, head_count, 2)
    diagonal_fading_multiplier = lax.dynamic_slice_in_dim(
        channel_group_fading_speed, first_head, head_count, 0
    )
    write_shift = math.log(4.0 * prompt_length / DK)
    beta = jax.nn.sigmoid(diagonal_speed_entries[:, 1, :] - write_shift)
    fading_exponent = (
        -diagonal_fading_multiplier[None, :] * jax.nn.softplus(diagonal_speed_entries[:, 0, :])
        + summed_shrink_logs
    )
    terms = block_terms(
        query.transpose(1, 0, 2),
        keys.transpose(1, 0, 2),
        values.transpose(1, 0, 2),
        fading_exponent.T,
        beta.T,
    )
    eye_heads = jnp.broadcast_to(jnp.eye(DK, dtype=jnp.float32), (head_count, DK, DK))
    zero_heads = jnp.zeros((head_count, DK, DK), jnp.float32)

    def local_step(carry, inputs):
        power, offset_state = carry
        u_i, w_i, qd_i, kd_i, a_i, gl_i = inputs
        w_power = jnp.einsum("hcd,hde->hce", w_i, power, precision=HIGH)
        v_zero = u_i - jnp.einsum("hcd,hde->hce", w_i, offset_state, precision=HIGH)
        base = jnp.einsum("hcd,hde->hce", qd_i, offset_state, precision=HIGH) + jnp.einsum(
            "hcs,hse->hce", a_i, v_zero, precision=HIGH
        )
        coupling = jnp.einsum("hcd,hde->hce", qd_i, power, precision=HIGH) - jnp.einsum(
            "hcs,hse->hce", a_i, w_power, precision=HIGH
        )
        power = power * gl_i[:, None, None] - jnp.einsum(
            "hcd,hce->hde", kd_i, w_power, precision=HIGH
        )
        offset_state = offset_state * gl_i[:, None, None] + jnp.einsum(
            "hcd,hce->hde", kd_i, v_zero, precision=HIGH
        )
        return ((power, offset_state), (base, coupling))

    inputs = tuple((jnp.moveaxis(t, 1, 0) for t in terms))
    (power, own_state), (base, coupling) = lax.scan(local_step, (eye_heads, zero_heads), inputs)
    packed = jnp.concatenate([power, own_state], axis=2)[None]
    every_piece = lax.all_gather(packed, "sp", axis=0, tiled=True)

    def walk(carry, piece):
        following = matmul_heads(piece[:, :, :DK], carry) + piece[:, :, DK:]
        return (following, carry)

    final_state, before = lax.scan(walk, zero_heads, every_piece)
    entry_state = lax.dynamic_index_in_dim(before, lax.axis_index("sp"), 0, keepdims=False)
    cache = final_state.astype(jnp.bfloat16)
    outputs = base + jnp.einsum("nhcd,hde->nhce", coupling, entry_state, precision=HIGH)
    heads_out = outputs.transpose(1, 0, 2, 3).reshape(head_count, tok_rows, DK).transpose(1, 0, 2)
    normed = heads_out * lax.rsqrt(jnp.mean(heads_out * heads_out, axis=-1, keepdims=True) + EPS)
    gate_rows = raw[3].reshape(tok_rows, head_count, DK).astype(jnp.float32)
    gated = normed * result_scaling_vector.astype(jnp.float32) * silu(gate_rows)
    mixed = gated.reshape(tok_rows, local_width).astype(jnp.bfloat16)
    unit_query = l2_unit(generated_probe_vector.astype(jnp.float32)) * DK ** (-0.5)
    new_read = jnp.einsum("nhd,hde->nhe", unit_query, cache.astype(jnp.float32), precision=HIGH)
    return (mixed, cache, new_read)


def solution(mesh):
    in_specs = (
        P("sp", "tp"),
        P(None, "tp"),
        P(None, "tp"),
        P(None, "tp"),
        P(None, "tp"),
        P(),
        P(None, None, "tp"),
        P(),
        P("sp", "tp"),
        P(),
        P("sp", "tp", None),
    )
    out_specs = (P("sp", "tp"), P("tp", None, None), P("sp", "tp", None))
    return jax.shard_map(
        on_device, mesh=mesh, in_specs=in_specs, out_specs=out_specs, check_vma=False
    )
```

profile of v0, /device:TPU:24, one launch (start us, length us, event | category | flops | bytes accessed | tf_op | source)
XLA Modules:
  0.0 392.3 jit_solution(7289248820536227078)
XLA Ops:
  7.2 2.3 broadcast_in_dim.65
  9.4 4.4 %all-to-all-start = ((bf16[8,384,256]{2,1,0:T(8,128)(2,1)}), bf16[8,384,256]{2,1,0:T(8,128)(2,1)S(1)}, u32[]{:S(2)}, u32[]{:S(2)}) async-start(bf16[8,384,256]{2,1,0:T(8,128)(2,1)} %broadcast_in_dim.65), calls=%async_computation | async-start | bytes 3145728 | tf_op jit(solution)/shard_map/all_to_all | solution.py:19
  15.4 20.0 %all-to-all-done = bf16[8,384,256]{2,1,0:T(8,128)(2,1)S(1)} async-done(((bf16[8,384,256]{2,1,0:T(8,128)(2,1)}), bf16[8,384,256]{2,1,0:T(8,128)(2,1)S(1)}, u32[]{:S(2)}, u32[]{:S(2)}) %all-to-all-start) | async-done | bytes 1572896 | tf_op jit(solution)/shard_map/all_to_all | solution.py:19
  35.4 1.2 copy-done.1
  36.6 1.6 copy.42
  40.9 3.5 collective-permute-start
  47.8 29.5 %custom-call.3 = f32[1,6,1,64,64]{3,4,2,1,0:T(8,128)S(1)} custom-call(f32[1,6,1,64,64]{4,3,2,1,0:T(8,128)S(1)} %fusion.57), custom_call_target="InvertDiagBlocksLowerTriangular" | custom-call | tf_op jit(solution)/shard_map/triangular_solve | solution.py:69
  79.6 28.9 %while.30 = (s32[]{:T(128)}, f32[1,128,128]{2,1,0:T(8,128)S(1)}, f32[1,128,128]{2,1,0:T(8,128)S(1)}, f32[6,1,64,128]{3,2,1,0:T(8,128)}, f32[6,1,64,128]{3,2,1,0:...) while((s32[]{:T(128)}, f32[1,128,128]{2,1,0:T(8,128)S(1)}, ...), condition=%wide.region_4.5_spmd.clone, body=%wide.region_3.4_spmd.clone.sunk | while | flops 88219648 | bytes 1215665 | solution.py:177
  82.5 0.9 fusion.168
  83.5 1.0 fusion.167
  87.4 0.9 fusion.168
  88.3 1.0 fusion.167
  92.2 0.9 fusion.168
  93.1 1.0 fusion.167
  97.0 0.9 fusion.168
  97.9 1.0 fusion.167
  101.8 0.9 fusion.168
  102.8 1.0 fusion.167
  106.6 0.9 fusion.168
  107.6 1.0 fusion.167
  110.6 156.0 %all-gather.3.cloned.1.call-done = f32[64,128,256]{2,1,0:T(8,128)} async-done(((f32[1,128,256]{2,1,0:T(8,128)}), f32[64,128,256]{2,1,0:T(8,128)}) %all-gather.3.cloned.1.call-update) | async-done | bytes 8388624 | tf_op jit(solution)/shard_map/all_gather | solution.py:179
  266.6 114.5 %while.31 = (s32[]{:T(128)}, f32[1,128,128]{2,1,0:T(8,128)S(1)}, f32[64,1,128,128]{3,2,1,0:T(8,128)}, f32[64,1,128,256]{3,2,1,0:T(8,128)}, s32[]{:T(128)}, /*index=5*/s32[]{:T(128)}) while((s32[]{:T(128)}, f32[1,128,128]{2,1,0:T(8,128)S(1)}, f32[64,1,128,128]{3,2,1,0:T(8,128)}, f32[64,1,128,256]{3,2,1,0:T(8,128)}, s32[]{:T(128)}, ...), condition=%wide.region_6.7_spmd.clone, body=%wide.region_5.6_spmd.clone.sunk | while | flops 25214980 | bytes 787028 | solution.py:185
  269.0 0.9 dynamic-slice_bitcast_fusion.3
  272.6 0.9 dynamic-slice_bitcast_fusion.3
  274.4 0.9 dynamic-slice_bitcast_fusion.3
  276.2 0.9 dynamic-slice_bitcast_fusion.3
  279.8 0.9 dynamic-slice_bitcast_fusion.3
  283.4 0.9 dynamic-slice_bitcast_fusion.3
  288.7 0.9 dynamic-slice_bitcast_fusion.3
  292.3 0.9 dynamic-slice_bitcast_fusion.3
  381.2 1.2 multiply_reduce_fusion
  383.2 2.3 fusion.69
  (365 shorter events, 133.3 us)
Async XLA Ops:
  7.2 31.0 %copy-start = (bf16[2048,128]{1,0:T(8,128)(2,1)S(1)}, bf16[2048,128]{1,0:T(8,128)(2,1)}, u32[]{:S(2)}) copy-start(bf16[2048,128]{1,0:T(8,128)(2,1)} %param.16) | copy-start | bytes 1572868
  9.4 4.5 %copy-start.11 = (f32[8]{0:T(128)S(1)}, f32[8]{0:T(128)}, u32[]{:S(2)}) copy-start(f32[8]{0:T(128)} %param.22) | copy-start | bytes 100
  9.4 5.8 %copy-start.8 = (bf16[3,4,128]{2,1,0:T(4,128)(2,1)S(1)}, bf16[3,4,128]{2,1,0:T(4,128)(2,1)}, u32[]{:S(2)}) copy-start(bf16[3,4,128]{2,1,0:T(4,128)(2,1)} %param.21) | copy-start | bytes 9220
  9.4 26.0 %all-to-all-start = ((bf16[8,384,256]{2,1,0:T(8,128)(2,1)}), bf16[8,384,256]{2,1,0:T(8,128)(2,1)S(1)}, u32[]{:S(2)}, u32[]{:S(2)}) async-start(bf16[8,384,256]{2,1,0:T(8,128)(2,1)} %broadcast_in_dim.65), calls=%async_computation | async-start | bytes 3145728 | tf_op jit(solution)/shard_map/all_to_all | solution.py:19
  13.9 252.7 %all-gather.3.cloned.1.call-start = ((), (), s32[]{:S(2)}) async-start(), calls=%async_computation.1 | async-start | bytes 8519680 | tf_op jit(solution)/shard_map/all_gather | solution.py:179
  35.4 1.2 copy-start.1
  38.2 1.0 copy-start.2
  39.2 1.0 copy-start.3
  40.3 4.1 %copy-start.7 = (bf16[2,2048,8]{1,2,0:T(8,128)(2,1)S(1)}, bf16[2,2048,8]{1,2,0:T(8,128)(2,1)}, u32[]{:S(2)}) copy-start(bf16[2,2048,8]{1,2,0:T(8,128)(2,1)} %param.20) | copy-start | bytes 196612
  40.3 4.6 %copy-start.9 = (f32[384,1]{0,1:T(1,128)S(1)}, f32[384,1]{0,1:T(1,128)}, u32[]{:S(2)}) copy-start(f32[384,1]{0,1:T(1,128)} %param.23) | copy-start | bytes 4612
  40.9 5.5 %collective-permute-start = (bf16[3,3,128]{2,1,0:T(4,128)(2,1)S(1)}, bf16[3,3,128]{2,1,0:T(4,128)(2,1)S(1)}, u32[]{:S(2)}, u32[]{:S(2)}) collective-permute-start(bf16[3,3,128]{2,1,0:T(4,128)(2,1)S(1)} %pad_maximum_fusion.1), channel_id=1, source_target_pairs={{0,8},{8,16},{16,24},{24,32},{32,40},{40,48},{48,56},{56,64},{64,7... | collective-permute-start | bytes 6920 | tf_op jit(solution)/shard_map/ppermute | solution.py:38
  79.6 29.7 %copy-start.12 = (bf16[128]{0:T(256)(128)(2,1)S(1)}, bf16[128]{0:T(256)(128)(2,1)}, u32[]{:S(2)}) copy-start(bf16[128]{0:T(256)(128)(2,1)} %param.24) | copy-start | bytes 772
  79.6 29.7 %copy-start.10 = (bf16[1,1,128]{2,1,0:T(2,128)(2,1)S(1)}, bf16[1,1,128]{2,1,0:T(2,128)(2,1)}, u32[]{:S(2)}) copy-start(bf16[1,1,128]{2,1,0:T(2,128)(2,1)} %param.25) | copy-start | bytes 772
  266.6 114.5 %copy-start.4 = (f32[6,1,64,128]{3,2,1,0:T(8,128)S(1)}, f32[6,1,64,128]{3,2,1,0:T(8,128)}, u32[]{:S(2)}) copy-start(f32[6,1,64,128]{3,2,1,0:T(8,128)} %get-tuple-element.86) | copy-start | bytes 589828
  266.6 114.5 %copy-start.5 = (f32[6,1,64,128]{3,2,1,0:T(8,128)S(1)}, f32[6,1,64,128]{3,2,1,0:T(8,128)}, u32[]{:S(2)}) copy-start(f32[6,1,64,128]{3,2,1,0:T(8,128)} %get-tuple-element.90) | copy-start | bytes 589828
  382.5 2.9 copy-start.6
Sparse Core Ops, SparseCore 0:
  109.4 157.2 all-gather.2
where the time goes:
time: 396 us; the launch traced here: 392 us
  waiting for transfers between devices  177 us (45%)
  other arithmetic  72.5 us (18%)
  local copies, waits for them, and re-layouts  69.4 us (18%)
  matrix products  47.2 us (12%)
  between operations  15.8 us (4%)
  starting transfers between devices  7.95 us (2%)
    all_gather x1, waiting for transfers between devices, on_device(): every_piece = lax.all_gather(packed, 'sp', axis=0, tiled=True)  156 us
    squeeze x64, local copies, waits for them, and re-layouts, on_device(): final_state, before = lax.scan(walk, zero_heads, every_piece)  58.4 us
    dynamic_update_slice x64, other arithmetic, on_device(): final_state, before = lax.scan(walk, zero_heads, every_piece)  40.2 us
    another operation x4, other arithmetic, block_terms(): lax.linalg.triangular_solve(eye + a_mat, jnp.broadcast_to(eye, a_mat.shap...  29.6 us
    all_to_all x1, waiting for transfers between devices, sent_to_all(): lax.all_to_all(jnp.broadcast_to(shard[None], (count, *shard.shape)), axis...  20 us
    dot_general x64, matrix products, matmul_heads(): return jnp.einsum('hij,hjk->hik', left, right, precision=HIGH)  13.2 us
  transfers between devices with their start and end apart: 3, of which 3 were waited for; matrix products, arithmetic and copies ran while one was open for 1% of the time, Pallas kernels for 0%

commit v1 on v0

v1 whole, which is shorter than its diff:
```python
import functools
import math

import jax
import jax.numpy as jnp
from jax import lax
from jax.experimental import pallas as pl
from jax.experimental.pallas import tpu as pltpu
from jax.sharding import PartitionSpec as P

DK = 128
CONV = 4
EPS = 1e-06
MESH = pl.DeviceIdType.MESH
F32 = jnp.float32
BF16 = jnp.bfloat16

ROWS = 128
RIM = 16


def silu(value):
    return value * jax.nn.sigmoid(value)


def halves(value):
    high = value.astype(BF16)
    low = (value - high.astype(F32)).astype(BF16)
    return high, low


def dot(left, right, dims):
    return lax.dot_general(left, right, dims, preferred_element_type=F32)


def dot3(left, right, dims):
    lh, ll = halves(left)
    rh, rl = halves(right)
    return dot(lh, rh, dims) + (dot(lh, rl, dims) + dot(ll, rh, dims))


NN = (((1,), (0,)), ((), ()))
TN = (((0,), (0,)), ((), ()))
BNN = (((2,), (1,)), ((0,), (0,)))
BNT = (((2,), (2,)), ((0,), (0,)))


def project_kernel(
    x_hbm, wq_hbm, wk_hbm, wv_hbm, wz_hbm, wr_hbm,
    raw_ref, rates_ref, rim_ref,
    x_all, w_all, w_rate, tail, rim_in,
    load_sem, send_sem, recv_sem, pass_sem, got_sem, rim_sem,
):
    sp = lax.axis_index("sp")
    tp = lax.axis_index("tp")
    n_sp = lax.axis_size("sp")
    chip, core = tp // 2, tp % 2
    partner = chip * 2 + (1 - core)
    rows, width = x_hbm.shape
    parts = rows // ROWS

    def columns(slot):
        return pl.ds(pl.multiple_of(slot * width, width), width)

    load_x = pltpu.make_async_copy(x_hbm, x_all.at[:, columns(tp)], load_sem.at[0])
    load_x.start()
    loads = []
    for i, w in enumerate((wq_hbm, wk_hbm, wv_hbm, wz_hbm)):
        loads.append(
            pltpu.make_async_copy(w, w_all.at[:, pl.ds(i * DK, DK)], load_sem.at[1 + i])
        )
    loads.append(pltpu.make_async_copy(wr_hbm, w_rate, load_sem.at[5]))
    for load in loads:
        load.start()

    after, before = (sp + 1) % n_sp, (sp + n_sp - 1) % n_sp
    barrier = pltpu.get_barrier_semaphore()
    for r in (2, 1, 3):
        peer = ((chip + r) % 4) * 2 + core
        pl.semaphore_signal(barrier, inc=1, device_id=(sp, peer), device_id_type=MESH)
    pl.semaphore_signal(barrier, inc=1, device_id=(sp, partner), device_id_type=MESH)
    pl.semaphore_signal(barrier, inc=1, device_id=(after, tp), device_id_type=MESH)
    pl.semaphore_signal(barrier, inc=1, device_id=(before, tp), device_id_type=MESH)
    load_x.wait()
    pl.semaphore_wait(barrier, 6)

    order = [parts - 1] + list(range(parts - 1))
    sends = {}

    def block(part, slot):
        return x_all.at[pl.ds(part * ROWS, ROWS), columns(slot)]

    for part in order:
        for r in (1, 3, 2):
            peer = ((chip + r) % 4) * 2 + core
            copy = pltpu.make_async_remote_copy(
                src_ref=block(part, tp), dst_ref=block(part, tp),
                send_sem=send_sem.at[part, r], recv_sem=recv_sem.at[part, r],
                device_id=(sp, peer), device_id_type=MESH,
            )
            copy.start()
            sends[part, r] = copy
        copy = pltpu.make_async_remote_copy(
            src_ref=block(part, tp), dst_ref=block(part, tp),
            send_sem=pass_sem.at[part, 0], recv_sem=got_sem.at[part, 0],
            device_id=(sp, partner), device_id_type=MESH,
        )
        copy.start()
        sends[part, 0] = copy

    for load in loads:
        load.wait()

    passes = []
    rim_copy = None
    for part in order:
        for r in (1, 3, 2):
            sends[part, r].wait_recv()
            slot = ((chip + 4 - r) % 4) * 2 + core
            copy = pltpu.make_async_remote_copy(
                src_ref=block(part, slot), dst_ref=block(part, slot),
                send_sem=pass_sem.at[part, r], recv_sem=got_sem.at[part, r],
                device_id=(sp, partner), device_id_type=MESH,
            )
            copy.start()
            passes.append(copy)
        sends[part, 0].wait_recv()
        for copy in passes[-3:]:
            copy.wait_recv()
        x = x_all[pl.ds(part * ROWS, ROWS), :]
        here = pl.ds(part * ROWS, ROWS)
        raw = dot(x, w_all[...], NN).astype(BF16)
        raw_ref[here, :] = raw
        if rim_copy is None:
            tail[...] = raw[ROWS - RIM :, : 3 * DK]
        rates_ref[0, here, :] = dot(x, w_rate[0], NN)
        rates_ref[1, here, :] = dot(x, w_rate[1], NN)
        if rim_copy is None:
            rim_copy = pltpu.make_async_remote_copy(
                src_ref=tail, dst_ref=rim_in,
                send_sem=rim_sem.at[0], recv_sem=rim_sem.at[1],
                device_id=(after, tp), device_id_type=MESH,
            )
            rim_copy.start()
    rim_copy.wait_recv()
    rim_ref[...] = rim_in[...]
    rim_copy.wait_send()
    for copy in sends.values():
        copy.wait_send()
    for copy in passes:
        copy.wait_send()


def project(x, wq, wk, wv, wz, wr):
    rows, width = x.shape
    depth = wq.shape[0]
    parts = rows // ROWS
    heads = wr.shape[2]
    any_space = pl.BlockSpec(memory_space=pl.ANY)
    vmem = pl.BlockSpec(memory_space=pltpu.VMEM)
    return pl.pallas_call(
        project_kernel,
        out_shape=(
            jax.ShapeDtypeStruct((rows, 4 * DK), BF16),
            jax.ShapeDtypeStruct((2, rows, heads), F32),
            jax.ShapeDtypeStruct((RIM, 3 * DK), BF16),
        ),
        in_specs=[any_space] * 6,
        out_specs=(vmem, vmem, vmem),
        scratch_shapes=[
            pltpu.VMEM((rows, depth), BF16),
            pltpu.VMEM((depth, 4 * DK), BF16),
            pltpu.VMEM((2, depth, heads), BF16),
            pltpu.VMEM((RIM, 3 * DK), BF16),
            pltpu.VMEM((RIM, 3 * DK), BF16),
            pltpu.SemaphoreType.DMA((6,)),
            pltpu.SemaphoreType.DMA((parts, 4)),
            pltpu.SemaphoreType.DMA((parts, 4)),
            pltpu.SemaphoreType.DMA((parts, 4)),
            pltpu.SemaphoreType.DMA((parts, 4)),
            pltpu.SemaphoreType.DMA((2,)),
        ],
        compiler_params=pltpu.CompilerParams(collective_id=0, has_side_effects=True),
    )(x, wq, wk, wv, wz, wr)


def inverse_of_unit_lower(a, row, col):
    eye = (row == col).astype(F32)
    size = 8
    y = jnp.where(row // size == col // size, a, 0.0)
    t = eye - y
    y2 = dot3(y, y, BNN)
    t, y4 = t + dot3(t, y2, BNN), dot3(y2, y2, BNN)
    t = t + dot3(t, y4, BNN)
    while size < ROWS:
        joins = (row // (2 * size) == col // (2 * size)) & (row // size != col // size)
        t = t - dot3(t, dot3(jnp.where(joins, a, 0.0), t, BNN), BNN)
        size *= 2
    return t


def scan_kernel(
    raw_ref, rates_ref, rim_ref, taps_ref, speed_ref, logs_ref, gain_ref, probe_ref,
    mixed_ref, cache_ref, read_ref,
    ext, board, own, send_sem, recv_sem,
):
    sp = lax.axis_index("sp")
    tp = lax.axis_index("tp")
    n_sp = lax.axis_size("sp")
    rows = raw_ref.shape[0]
    parts = rows // ROWS
    strides = (1, 4, 16)

    def member(level, turn):
        stride = strides[level]
        digit = (sp // stride) % 4
        return sp + ((digit + turn) % 4 - digit) * stride

    barrier = pltpu.get_barrier_semaphore()
    for level in (2, 1, 0):
        for turn in (2, 1, 3):
            pl.semaphore_signal(
                barrier, inc=1, device_id=(member(level, turn), tp), device_id_type=MESH
            )

    first = (sp == 0).astype(F32)
    ext[pl.ds(0, RIM), :] = rim_ref[...].astype(F32) * (1.0 - first)
    ext[pl.ds(RIM, rows), :] = raw_ref[:, : 3 * DK].astype(F32)
    outs = []
    for c in range(3):
        lanes = pl.ds(c * DK, DK)
        total = jnp.zeros((rows, DK), F32)
        for lag in range(CONV):
            tap = taps_ref[c, pl.ds(lag, 1), :].astype(F32)
            total = total + tap * ext[pl.ds(RIM - (CONV - 1) + lag, rows), lanes]
        outs.append(silu(total))
    query, keys, values = outs
    query = query * (lax.rsqrt(jnp.sum(query * query, axis=-1, keepdims=True) + EPS) * DK**-0.5)
    keys = keys * lax.rsqrt(jnp.sum(keys * keys, axis=-1, keepdims=True) + EPS)

    heads = rates_ref.shape[2]
    mine = lax.broadcasted_iota(jnp.int32, (rows, heads), 1) == tp
    fade = jnp.sum(jnp.where(mine, rates_ref[0], 0.0), axis=-1, keepdims=True)
    write = jnp.sum(jnp.where(mine, rates_ref[1], 0.0), axis=-1, keepdims=True)
    beta = jax.nn.sigmoid(write - math.log(4.0 * rows * n_sp / DK))
    soft = jnp.maximum(fade, 0.0) + jnp.log1p(jnp.exp(-jnp.abs(fade)))
    exponent = logs_ref[...] - speed_ref[tp] * soft

    shape = (parts, ROWS, DK)
    row = lax.broadcasted_iota(jnp.int32, (ROWS, ROWS), 0)
    col = lax.broadcasted_iota(jnp.int32, (ROWS, ROWS), 1)
    eye = (row == col).astype(F32)
    below = (row >= col).astype(BF16)
    spread = jnp.broadcast_to(exponent, (rows, DK)).reshape(shape)
    summed = []
    for part in range(parts):
        high, low = halves(spread[part])
        lowest = (spread[part] - high.astype(F32) - low.astype(F32)).astype(BF16)
        summed.append(dot(below, high, NN) + (dot(below, low, NN) + dot(below, lowest, NN)))
    decay = jnp.stack([jnp.exp(jnp.where(row >= col, s - s.T, -1e30)) for s in summed])
    summed = jnp.stack(summed)
    query, keys, values = (a.reshape(shape) for a in (query, keys, values))
    beta = beta.reshape(parts, ROWS, 1)

    k_beta = keys * beta
    a_mat = jnp.where((row > col)[None], dot3(k_beta, keys, BNT) * decay, 0.0)
    t_mat = inverse_of_unit_lower(a_mat, row[None], col[None])
    grown = jnp.exp(summed)
    right = jnp.concatenate([k_beta * grown, values * beta], axis=2)
    wu = dot3(t_mat, right, BNN)
    k_dec = keys * jnp.exp(summed[:, ROWS - 1 :, :] - summed)
    last = grown[:, ROWS - 1 :, :]

    news, starts, gains = [], [], []
    m = None
    gain = jnp.ones((1, DK), F32)
    for part in range(parts):
        w = wu[part, :, :DK]
        new = jnp.concatenate([gain * w, wu[part, :, DK:]], axis=1)
        if m is not None:
            new = new - dot3(w, m, NN)
        news.append(new)
        starts.append(m)
        gains.append(gain)
        step = dot3(k_dec[part], new, TN)
        twice = jnp.concatenate([last[part], last[part]], axis=1)
        m = step if m is None else twice * m + step
        gain = gain * last[part]

    def post(level, m, gain):
        digit = (sp // strides[level]) % 4
        g2 = jnp.concatenate([gain, gain], axis=1)
        high = g2.astype(BF16).astype(F32)
        mid = (g2 - high).astype(BF16).astype(F32)
        low = g2 - high - mid
        at = lax.broadcasted_iota(jnp.int32, (RIM, 2 * DK), 0)
        extra = jnp.where(at == 0, high, jnp.where(at == 1, mid, jnp.where(at == 2, low, 0.0)))
        board[level, digit, pl.ds(0, DK), :] = m.astype(BF16)
        board[level, digit, pl.ds(DK, RIM), :] = extra.astype(BF16)
        copies = []
        for turn in (2, 1, 3):
            place = board.at[level, digit]
            copy = pltpu.make_async_remote_copy(
                src_ref=place, dst_ref=place,
                send_sem=send_sem.at[level, turn], recv_sem=recv_sem.at[level, turn],
                device_id=(member(level, turn), tp), device_id_type=MESH,
            )
            copy.start()
            copies.append(copy)
        return copies

    def read(level, i):
        transition = board[level, i, pl.ds(0, DK), pl.ds(0, DK)]
        whole = board[level, i, pl.ds(0, DK), :].astype(F32)
        extra = board[level, i, pl.ds(DK, RIM), :].astype(F32)
        return transition, whole, extra[0:1] + extra[1:2] + extra[2:3]

    def apply(transition, g2, m):
        high, low = halves(m)
        return g2 * m - (dot(transition, high, NN) + dot(transition, low, NN))

    def compose(level):
        digit = (sp // strides[level]) % 4
        _, m, gain = read(level, 0)
        before, before_gain = jnp.zeros((DK, 2 * DK), F32), jnp.ones((1, 2 * DK), F32)
        for i in range(1, 4):
            before = jnp.where(digit == i, m, before)
            before_gain = jnp.where(digit == i, gain, before_gain)
            transition, own_m, g2 = read(level, i)
            scaled = jnp.concatenate([gain[:, :DK] * own_m[:, :DK], own_m[:, DK:]], axis=1)
            m = apply(transition, g2, m) + scaled
            gain = gain * g2
        return m, gain[:, :DK], before, before_gain[:, :DK]

    pl.semaphore_wait(barrier, 9)
    copies = post(0, m, gain)

    base, coupling = [], []
    attend = dot3(query, keys, BNT) * decay
    q_dec = query * grown
    for part in range(parts):
        both = dot3(attend[part], news[part], NN)
        if starts[part] is not None:
            both = both + dot3(q_dec[part], starts[part], NN)
        coupling.append(gains[part] * q_dec[part] - both[:, :DK])
        base.append(both[:, DK:])
    coupling = jnp.concatenate(coupling, axis=0)
    base = jnp.concatenate(base, axis=0)
    gate = silu(raw_ref[:, 3 * DK :].astype(F32)) * gain_ref[...].astype(F32)

    sent = list(copies)
    for level in range(2):
        for copy in copies:
            copy.wait_recv()
        m, gain, before, before_gain = compose(level)
        copies = post(level + 1, m, gain)
        sent += copies
        both = dot3(coupling, before, NN)
        coupling = before_gain * coupling - both[:, :DK]
        base = base + both[:, DK:]
    for copy in copies:
        copy.wait_recv()

    digit = (sp // strides[2]) % 4
    state = board[2, 0, pl.ds(0, DK), pl.ds(DK, DK)].astype(F32)
    entry = jnp.zeros((DK, DK), F32)
    for i in range(1, 4):
        entry = jnp.where(digit == i, state, entry)
        transition, whole, g2 = read(2, i)
        state = apply(transition, g2[:, :DK], state) + whole[:, DK:]
    out = base + dot3(coupling, entry, NN)
    normed = out * lax.rsqrt(jnp.mean(out * out, axis=-1, keepdims=True) + EPS)
    mixed_ref[...] = (normed * gate).astype(BF16)
    cache = state.astype(BF16)
    cache_ref[0] = cache
    probe = probe_ref[0].astype(F32)
    probe = probe * (lax.rsqrt(jnp.sum(probe * probe, axis=-1, keepdims=True) + EPS) * DK**-0.5)
    high, low = halves(jnp.broadcast_to(probe, (16, DK)))
    read_ref[0] = (dot(high, cache, NN) + dot(low, cache, NN))[0:1]
    for copy in sent:
        copy.wait_send()


def scan(raw, rates, rim, taps, speed, logs, gain, probe):
    rows = raw.shape[0]
    vmem = pl.BlockSpec(memory_space=pltpu.VMEM)
    smem = pl.BlockSpec(memory_space=pltpu.SMEM)
    return pl.pallas_call(
        scan_kernel,
        out_shape=(
            jax.ShapeDtypeStruct((rows, DK), BF16),
            jax.ShapeDtypeStruct((1, DK, DK), BF16),
            jax.ShapeDtypeStruct((1, 1, DK), F32),
        ),
        in_specs=[vmem, vmem, vmem, vmem, smem, vmem, vmem, vmem],
        out_specs=(vmem, vmem, vmem),
        scratch_shapes=[
            pltpu.VMEM((rows + RIM, 3 * DK), F32),
            pltpu.VMEM((3, 4, DK + RIM, 2 * DK), BF16),
            pltpu.VMEM((8, DK), F32),
            pltpu.SemaphoreType.DMA((3, 4)),
            pltpu.SemaphoreType.DMA((3, 4)),
        ],
        compiler_params=pltpu.CompilerParams(collective_id=1, has_side_effects=True),
    )(raw, rates, rim, taps, speed, logs, gain, probe)


def on_device(x, wq, wk, wv, wz, wr, taps, speed, logs, gain, probe):
    raw, rates, rim = project(x, wq, wk, wv, wz, wr)
    return scan(raw, rates, rim, taps, speed, logs, gain.reshape(1, DK), probe)


def solution(mesh):
    in_specs = (
        P("sp", "tp"),
        P(None, "tp"),
        P(None, "tp"),
        P(None, "tp"),
        P(None, "tp"),
        P(),
        P(None, None, "tp"),
        P(),
        P("sp", "tp"),
        P(),
        P("sp", "tp", None),
    )
    out_specs = (P("sp", "tp"), P("tp", None, None), P("sp", "tp", None))
    return jax.shard_map(
        on_device, mesh=mesh, in_specs=in_specs, out_specs=out_specs, check_vma=False
    )
```

time: 396 us -> 73.1 us (0.18)
  the two profiles are of different devices: /device:TPU:24 before, /device:TPU:64 now
where the time goes in v1:
time: 73.1 us; the launch traced here: 72.9 us
  Pallas kernels  65.9 us (90%)
  local copies, waits for them, and re-layouts  6.32 us (9%)
    pallas_call x1, Pallas kernels, scan(): pl.pallas_call(scan_kernel, out_shape=(jax.ShapeDtypeStruct((rows, DK), B...  47.3 us
    pallas_call x1, Pallas kernels, project(): pl.pallas_call(project_kernel, out_shape=(jax.ShapeDtypeStruct((rows, 4 *...  18.6 us
    unnamed x11, local copies, waits for them, and re-layouts  6.32 us

profile of v1, /device:TPU:64, one launch (start us, length us, event | category | flops | bytes accessed | tf_op | source)
XLA Modules:
  0.0 72.9 jit_solution(14583666620502318644)
XLA Ops:
  0.6 2.1 %copy.14.wr_hbm = bf16[2,2048,8]{2,1,0:T(8,128)(2,1)} copy(bf16[2,2048,8]{1,2,0:T(8,128)(2,1)} %param.16) | data formatting | bytes 131072 | tf_op args[5]
  2.8 18.6 %shard_map.130 = (bf16[384,512]{1,0:T(8,128)(2,1)}, f32[2,384,8]{2,1,0:T(8,128)}, bf16[16,384]{1,0:T(8,128)(2,1)}) custom-call(bf16[384,256]{1,0:T(8,128)(2,1)} %x_hbm.1, bf16[2048,128]{1,0:T(8,128)(2,1)} %wq_hbm.1, bf16[2048,128]{1,0:T(8,128)(2,1)} %wk_hbm.1, bf16[2048,128]{1,0:T(8,128)(2,1)} %wv_hbm.1, bf16[2048,128]{1,0:T(8,128)(2,1)} %wz_hbm.1, ...), custom_call_target="tpu_custom_call" | custom-call | tf_op jit(solution)/shard_map/pallas_call | solution.py:161
  21.3 0.0 copy-start.1
  21.4 0.7 copy-done.1
  22.0 0.8 %copy.15.logs_ref = f32[384,1]{1,0:T(8,128)} copy(f32[384,1]{0,1:T(1,128)S(1)} %copy-done.1) | data formatting | bytes 3072 | tf_op args[8]
  22.9 47.3 %shard_map.131 = (bf16[384,128]{1,0:T(8,128)(2,1)}, bf16[1,128,128]{2,1,0:T(8,128)(2,1)}, f32[1,1,128]{2,1,0:T(1,128)}) custom-call(bf16[384,512]{1,0:T(8,128)(2,1)} %get-tuple-element.6.raw_ref, f32[2,384,8]{2,1,0:T(8,128)} %get-tuple-element.7.rates_ref, bf16[16,384]{1,0:T(8,128)(2,1)} %get-tuple-element.8.rim_ref, bf16[3,4,128]{2,1,0:T(4,128)(2,1)} %taps_ref.1, ...), custom_call_target="tpu_custom_call" | custom-call | tf_op jit(solution)/shard_map/pallas_call | solution.py:388
  70.2 0.0 copy-start
  70.2 1.5 %copy.19 = bf16[384,128]{1,0:T(8,128)(2,1)} copy(bf16[384,128]{1,0:T(8,128)(2,1)} %get-tuple-element.12) | data formatting | bytes 196608
  71.7 0.0 copy-done
  71.7 0.0 copy-start.2
  71.7 0.6 copy.20
  72.3 0.0 copy-done.2
  72.3 0.5 copy.21
Async XLA Ops:
  21.3 0.7 copy-start.1
  70.2 1.6 %copy-start = (bf16[1,128,128]{2,1,0:T(8,128)(2,1)S(1)}, bf16[1,128,128]{2,1,0:T(8,128)(2,1)}, u32[]{:S(2)}) copy-start(bf16[1,128,128]{2,1,0:T(8,128)(2,1)} %get-tuple-element.13) | copy-start | bytes 98308
  71.7 0.6 copy-start.2

commit v2 on v1

v2 whole, which is shorter than its diff:
```python
import functools
import math

import jax
import jax.numpy as jnp
from jax import lax
from jax.experimental import pallas as pl
from jax.experimental.pallas import tpu as pltpu
from jax.sharding import PartitionSpec as P

DK = 128
CONV = 4
EPS = 1e-06
MESH = pl.DeviceIdType.MESH
F32 = jnp.float32
BF16 = jnp.bfloat16

ROWS = 128
RIM = 16
EXTRA = 8
TOKENS = True
SHARE = DK // 4


def silu(value):
    return value * jax.nn.sigmoid(value)


def halves(value):
    high = value.astype(BF16)
    low = (value - high.astype(F32)).astype(BF16)
    return high, low


def dot(left, right, dims):
    return lax.dot_general(left, right, dims, preferred_element_type=F32)


def dot3(left, right, dims):
    lh, ll = halves(left)
    rh, rl = halves(right)
    return dot(lh, rh, dims) + (dot(lh, rl, dims) + dot(ll, rh, dims))


def dot2(left, right, dims):
    lh, ll = halves(left)
    right = right.astype(BF16)
    left = jnp.concatenate([lh, ll], axis=-1)
    return dot(left, jnp.concatenate([right, right], axis=-2), dims)


NN = (((1,), (0,)), ((), ()))
NT = (((1,), (1,)), ((), ()))
TN = (((0,), (0,)), ((), ()))
BNN = (((2,), (1,)), ((0,), (0,)))
BNT = (((2,), (2,)), ((0,), (0,)))


def inverse_of_unit_lower(a, row, col):
    eye = (row == col).astype(F32)
    size = 8
    y = jnp.where(row // size == col // size, a, 0.0)
    t = eye - y
    y2 = dot3(y, y, BNN)
    t, y4 = t + dot3(t, y2, BNN), dot3(y2, y2, BNN)
    t = t + dot3(t, y4, BNN)
    while size < ROWS:
        joins = (row // (2 * size) == col // (2 * size)) & (row // size != col // size)
        t = t - dot2(t, dot2(jnp.where(joins, a, 0.0), t, BNN), BNN)
        size *= 2
    return t


def kernel(
    x_hbm, wq_hbm, wk_hbm, wv_hbm, wz_hbm, wr_hbm,
    taps_ref, speed_ref, logs_ref, gain_ref, probe_ref,
    mixed_ref, cache_ref, read_ref,
    x_all, x_tail, w_all, w_rate, tail, rim_in, ext, gates,
    q_ref, k_ref, kb_ref, vb_ref, a_ref, sum_ref, decay_ref,
    board_0, board_1, board_2,
    load_sem, near_send, near_recv, core_send, core_recv, rim_sem,
    send_sem, recv_sem, pass_sem, got_sem, token,
):
    sp = lax.axis_index("sp")
    tp = lax.axis_index("tp")
    n_sp = lax.axis_size("sp")
    chip, core = tp // 2, tp % 2
    partner = chip * 2 + (1 - core)
    rows, width = x_hbm.shape
    parts = rows // ROWS
    strides, counts = (1, 4, 8), (4, 2, n_sp // 8)
    far = counts[2]
    digits = [(sp // stride) % count for stride, count in zip(strides, counts)]
    turns = [
        (2, 1, 3),
        (1,),
        sorted(range(1, far), key=lambda turn: min(turn, far - turn)),
    ]

    def member(level, turn):
        digit = digits[level]
        return sp + ((digit + turn) % counts[level] - digit) * strides[level]

    def columns(slot):
        return pl.ds(pl.multiple_of(slot * width, width), width)

    def near(r):
        return ((chip + r) % 4) * 2 + core

    load_x = pltpu.make_async_copy(x_hbm, x_all.at[:, columns(tp)], load_sem.at[0])
    load_x.start()
    load_tail = pltpu.make_async_copy(
        x_hbm.at[pl.ds(rows - RIM, RIM), :], x_tail.at[:, columns(tp)], load_sem.at[6]
    )
    load_tail.start()
    loads = []
    for i, w in enumerate((wq_hbm, wk_hbm, wv_hbm, wz_hbm)):
        loads.append(
            pltpu.make_async_copy(w, w_all.at[:, pl.ds(i * DK, DK)], load_sem.at[1 + i])
        )
    loads.append(pltpu.make_async_copy(wr_hbm, w_rate, load_sem.at[5]))
    for load in loads:
        load.start()

    after, before_sp = (sp + 1) % n_sp, (sp + n_sp - 1) % n_sp
    barrier = pltpu.get_barrier_semaphore()
    greeted = [(sp, near(r)) for r in (2, 1, 3)] + [(sp, partner), (after, tp), (before_sp, tp)]
    greeted += [(member(0, turn), tp) for turn in turns[0]] + [(member(1, 1), tp)]
    beyond = (1, far - 1) if TOKENS else turns[2]
    greeted += [(member(2, turn), tp) for turn in beyond]
    for peer in greeted:
        pl.semaphore_signal(barrier, inc=1, device_id=peer, device_id_type=MESH)
    load_x.wait()
    load_tail.wait()
    pl.semaphore_wait(barrier, len(greeted))

    def pass_token(i):
        if TOKENS and 0 < i < far // 2:
            pl.semaphore_wait(token.at[i - 1], 2)
        if TOKENS and i < far // 2 - 1:
            for turn in (1, far - 1):
                pl.semaphore_signal(
                    token.at[i], inc=1, device_id=(member(2, turn), tp), device_id_type=MESH
                )

    def block(part, slot):
        if part == parts:
            return x_tail.at[:, columns(slot)]
        return x_all.at[pl.ds(part * ROWS, ROWS), columns(slot)]

    def to(place, peer, send, recv):
        copy = pltpu.make_async_remote_copy(
            src_ref=place, dst_ref=place, send_sem=send, recv_sem=recv,
            device_id=(sp, peer), device_id_type=MESH,
        )
        copy.start()
        return copy

    sends, passes = {}, []
    order = [parts] + list(range(parts))
    for part in order:
        for r in (2, 1, 3):
            sends[part, r] = to(
                block(part, tp), near(r), near_send.at[part, r], near_recv.at[part, r]
            )
        sends[part, 0] = to(
            block(part, tp), partner, core_send.at[part, 0], core_recv.at[part, 0]
        )
    pass_token(0)
    for load in loads:
        load.wait()

    def gathered(part):
        mine = []
        for r in (1, 3, 2):
            sends[part, r].wait_recv()
            slot = ((chip + 4 - r) % 4) * 2 + core
            mine.append(
                to(block(part, slot), partner, core_send.at[part, r], core_recv.at[part, r])
            )
        sends[part, 0].wait_recv()
        for copy in mine:
            copy.wait_recv()
        passes.extend(mine)

    gathered(parts)
    tail[...] = dot(x_tail[...], w_all[:, pl.ds(0, 3 * DK)], NN).astype(BF16)
    rim_copy = pltpu.make_async_remote_copy(
        src_ref=tail, dst_ref=rim_in, send_sem=rim_sem.at[0], recv_sem=rim_sem.at[1],
        device_id=(after, tp), device_id_type=MESH,
    )
    rim_copy.start()
    pass_token(1)

    row = lax.broadcasted_iota(jnp.int32, (ROWS, ROWS), 0)
    col = lax.broadcasted_iota(jnp.int32, (ROWS, ROWS), 1)
    eye = (row == col).astype(F32)
    below = (row >= col).astype(BF16)
    gain_row = gain_ref[...].astype(F32)

    def prepare(part):
        here = pl.ds(part * ROWS, ROWS)
        x = x_all[here, :]
        raw = dot(x, w_all[...], NN).astype(BF16).astype(F32)
        rates = dot(x, w_rate[...], NT)
        ext[pl.ds(RIM + part * ROWS, ROWS), :] = raw[:, : 3 * DK]
        gates[here, :] = silu(raw[:, 3 * DK :]) * gain_row
        outs = []
        for c in range(3):
            lanes = pl.ds(c * DK, DK)
            total = jnp.zeros((ROWS, DK), F32)
            for lag in range(CONV):
                tap = taps_ref[c, pl.ds(lag, 1), :].astype(F32)
                total = total + tap * ext[
                    pl.ds(part * ROWS + RIM - (CONV - 1) + lag, ROWS), lanes
                ]
            outs.append(silu(total))
        query, keys, values = outs
        query = query * (
            lax.rsqrt(jnp.sum(query * query, axis=-1, keepdims=True) + EPS) * DK**-0.5
        )
        keys = keys * lax.rsqrt(jnp.sum(keys * keys, axis=-1, keepdims=True) + EPS)
        kinds = rates.shape[1]
        kind = lax.broadcasted_iota(jnp.int32, (ROWS, kinds), 1)
        fade = jnp.sum(jnp.where(kind == tp, rates, 0.0), axis=-1, keepdims=True)
        write = jnp.sum(jnp.where(kind == tp + kinds // 2, rates, 0.0), axis=-1, keepdims=True)
        beta = jax.nn.sigmoid(write - math.log(4.0 * rows * n_sp / DK))
        soft = jnp.maximum(fade, 0.0) + jnp.log1p(jnp.exp(-jnp.abs(fade)))
        spread = jnp.broadcast_to(logs_ref[:, here], (ROWS, ROWS)).T - speed_ref[tp] * soft
        high, low = halves(spread)
        lowest = (spread - high.astype(F32) - low.astype(F32)).astype(BF16)
        summed = dot(below, high, NN) + (dot(below, low, NN) + dot(below, lowest, NN))
        decay = jnp.exp(jnp.where(row >= col, summed - summed.T, -1e30))
        k_beta = keys * beta
        q_ref[part] = query
        k_ref[part] = keys
        kb_ref[part] = k_beta
        vb_ref[part] = values * beta
        sum_ref[part] = summed
        decay_ref[part] = decay
        a_ref[part] = jnp.where(row > col, dot3(k_beta, keys, NT) * decay, 0.0)

    for part in range(parts):
        gathered(part)
        if part == 0:
            rim_copy.wait_recv()
            ext[pl.ds(0, RIM), :] = jnp.where(sp == 0, 0.0, rim_in[...].astype(F32))
        prepare(part)
        pass_token(part + 2)

    query, keys, k_beta, summed, decay = (
        ref[...] for ref in (q_ref, k_ref, kb_ref, sum_ref, decay_ref)
    )
    t_mat = inverse_of_unit_lower(a_ref[...], row[None], col[None])
    grown = jnp.exp(summed)
    right = jnp.concatenate([k_beta * grown, vb_ref[...]], axis=2)
    wu = dot3(t_mat, right, BNN)
    k_dec = keys * jnp.exp(summed[:, ROWS - 1 :, :] - summed)
    last = grown[:, ROWS - 1 :, :]

    news, starts, gains = [], [], []
    m = None
    gain = jnp.ones((1, DK), F32)
    for part in range(parts):
        w = wu[part, :, :DK]
        new = jnp.concatenate([gain * w, wu[part, :, DK:]], axis=1)
        if m is not None:
            new = new - dot3(w, m, NN)
        news.append(new)
        starts.append(m)
        gains.append(gain)
        step = dot3(k_dec[part], new, TN)
        twice = jnp.concatenate([last[part], last[part]], axis=1)
        m = step if m is None else twice * m + step
        gain = gain * last[part]

    def gain_rows(gain):
        g2 = jnp.concatenate([gain, gain], axis=1)
        high = g2.astype(BF16).astype(F32)
        mid = (g2 - high).astype(BF16).astype(F32)
        low = g2 - high - mid
        at = lax.broadcasted_iota(jnp.int32, (EXTRA, 2 * DK), 0)
        extra = jnp.where(at == 0, high, jnp.where(at == 1, mid, jnp.where(at == 2, low, 0.0)))
        return extra.astype(BF16)

    def gain_of(extra):
        extra = extra.astype(F32)
        return extra[0:1] + extra[1:2] + extra[2:3]

    boards = (board_0, board_1)

    def remote(place, level, turn, send, recv):
        copy = pltpu.make_async_remote_copy(
            src_ref=place, dst_ref=place, send_sem=send, recv_sem=recv,
            device_id=(member(level, turn), tp), device_id_type=MESH,
        )
        copy.start()
        return copy

    def post(level, m, gain):
        board, digit = boards[level], digits[level]
        board[digit, pl.ds(0, DK), :] = m.astype(BF16)
        board[digit, pl.ds(DK, EXTRA), :] = gain_rows(gain)
        return [
            remote(
                board.at[digit], level, turn,
                send_sem.at[level, turn], recv_sem.at[level, turn],
            )
            for turn in turns[level]
        ]

    def post_quarters(m, gain):
        rounded, extra = m.astype(BF16), gain_rows(gain)
        for i in range(4):
            board_2[digits[2], i, pl.ds(0, SHARE), :] = rounded[i * SHARE : (i + 1) * SHARE]
            board_2[digits[2], i, pl.ds(SHARE, EXTRA), :] = extra
        place = board_2.at[digits[2], digits[0]]
        return {
            turn: remote(place, 2, turn, send_sem.at[2, turn], recv_sem.at[2, turn])
            for turn in turns[2]
        }

    def read(level, i):
        board = boards[level]
        transition = board[i, pl.ds(0, DK), pl.ds(0, DK)]
        whole = board[i, pl.ds(0, DK), :].astype(F32)
        return transition, whole, gain_of(board[i, pl.ds(DK, EXTRA), :])

    def apply(transition, g2, m):
        high, low = halves(m)
        wide = jnp.concatenate([transition, transition], axis=1)
        return g2 * m - dot(wide, jnp.concatenate([high, low], axis=0), NN)

    def compose(level):
        digit = digits[level]
        _, m, gain = read(level, 0)
        before, before_gain = jnp.zeros((DK, 2 * DK), F32), jnp.ones((1, 2 * DK), F32)
        for i in range(1, counts[level]):
            before = jnp.where(digit == i, m, before)
            before_gain = jnp.where(digit == i, gain, before_gain)
            transition, own_m, g2 = read(level, i)
            scaled = jnp.concatenate([gain[:, :DK] * own_m[:, :DK], own_m[:, DK:]], axis=1)
            m = apply(transition, g2, m) + scaled
            gain = gain * g2
        return m, gain[:, :DK], before, before_gain[:, :DK]

    copies = post(0, m, gain)

    base, coupling = [], []
    attend = dot3(query, keys, BNT) * decay
    q_dec = query * grown
    for part in range(parts):
        both = dot3(attend[part], news[part], NN)
        if starts[part] is not None:
            both = both + dot3(q_dec[part], starts[part], NN)
        coupling.append(gains[part] * q_dec[part] - both[:, :DK])
        base.append(both[:, DK:])
    coupling = jnp.concatenate(coupling, axis=0)
    base = jnp.concatenate(base, axis=0)

    sent = list(copies)
    for level in range(2):
        for copy in copies:
            copy.wait_recv()
        m, gain, before, before_gain = compose(level)
        if level == 0:
            copies = post(1, m, gain)
            sent += copies
        else:
            quarters = post_quarters(m, gain)
            sent += list(quarters.values())
        both = dot3(coupling, before, NN)
        coupling = before_gain * coupling - both[:, :DK]
        base = base + both[:, DK:]
    passed = []
    for turn in turns[2]:
        quarters[turn].wait_recv()
        place = board_2.at[(digits[2] + far - turn) % far, digits[0]]
        for side in turns[0]:
            passed.append(
                remote(place, 0, side, pass_sem.at[turn, side], got_sem.at[turn, side])
            )
    for copy in passed:
        copy.wait_recv()
    sent += passed

    def part_of(i, lanes):
        return board_2[i, :, pl.ds(0, SHARE), lanes].reshape(DK, DK)

    state = part_of(0, pl.ds(DK, DK)).astype(F32)
    entry = jnp.zeros((DK, DK), F32)
    for i in range(1, far):
        entry = jnp.where(digits[2] == i, state, entry)
        g2 = gain_of(board_2[i, 0, pl.ds(SHARE, EXTRA), pl.ds(0, DK)])
        added = part_of(i, pl.ds(DK, DK)).astype(F32)
        state = apply(part_of(i, pl.ds(0, DK)), g2, state) + added
    out = base + dot3(coupling, entry, NN)
    normed = out * lax.rsqrt(jnp.mean(out * out, axis=-1, keepdims=True) + EPS)
    mixed_ref[...] = (normed * gates[...]).astype(BF16)
    cache = state.astype(BF16)
    cache_ref[0] = cache
    probe = probe_ref[0].astype(F32)
    probe = probe * (lax.rsqrt(jnp.sum(probe * probe, axis=-1, keepdims=True) + EPS) * DK**-0.5)
    high, low = halves(jnp.broadcast_to(probe, (16, DK)))
    read_ref[0] = (dot(high, cache, NN) + dot(low, cache, NN))[0:1]
    rim_copy.wait_send()
    for copy in sent + passes + list(sends.values()):
        copy.wait_send()


def fused(x, wq, wk, wv, wz, wr, taps, speed, logs, gain, probe):
    rows = x.shape[0]
    depth = wq.shape[0]
    parts = rows // ROWS
    any_space = pl.BlockSpec(memory_space=pl.ANY)
    vmem = pl.BlockSpec(memory_space=pltpu.VMEM)
    smem = pl.BlockSpec(memory_space=pltpu.SMEM)
    dma = pltpu.SemaphoreType.DMA
    block = pltpu.VMEM((parts, ROWS, DK), F32)
    return pl.pallas_call(
        kernel,
        out_shape=(
            jax.ShapeDtypeStruct((rows, DK), BF16),
            jax.ShapeDtypeStruct((1, DK, DK), BF16),
            jax.ShapeDtypeStruct((1, 1, DK), F32),
        ),
        in_specs=[any_space] * 6 + [vmem, smem, vmem, vmem, vmem],
        out_specs=(vmem, vmem, vmem),
        scratch_shapes=[
            pltpu.VMEM((rows, depth), BF16),
            pltpu.VMEM((RIM, depth), BF16),
            pltpu.VMEM((depth, 4 * DK), BF16),
            pltpu.VMEM(wr.shape, BF16),
            pltpu.VMEM((RIM, 3 * DK), BF16),
            pltpu.VMEM((RIM, 3 * DK), BF16),
            pltpu.VMEM((rows + RIM, 3 * DK), F32),
            pltpu.VMEM((rows, DK), F32),
            *[block] * 7,
            pltpu.VMEM((4, DK + EXTRA, 2 * DK), BF16),
            pltpu.VMEM((2, DK + EXTRA, 2 * DK), BF16),
            pltpu.VMEM((8, 4, SHARE + EXTRA, 2 * DK), BF16),
            dma((7,)),
            dma((parts + 1, 4)),
            dma((parts + 1, 4)),
            dma((parts + 1, 4)),
            dma((parts + 1, 4)),
            dma((2,)),
            dma((3, 8)),
            dma((3, 8)),
            dma((8, 4)),
            dma((8, 4)),
            pltpu.SemaphoreType.REGULAR((4,)),
        ],
        compiler_params=pltpu.CompilerParams(collective_id=0, has_side_effects=True),
    )(x, wq, wk, wv, wz, wr, taps, speed, logs, gain, probe)


def on_device(x, wq, wk, wv, wz, wr, taps, speed, logs, gain, probe):
    by_kind = wr.transpose(0, 2, 1).reshape(-1, wr.shape[1])
    return fused(
        x, wq, wk, wv, wz, by_kind, taps, speed, logs.reshape(1, -1), gain.reshape(1, DK), probe
    )


def solution(mesh):
    in_specs = (
        P("sp", "tp"),
        P(None, "tp"),
        P(None, "tp"),
        P(None, "tp"),
        P(None, "tp"),
        P(),
        P(None, None, "tp"),
        P(),
        P("sp", "tp"),
        P(),
        P("sp", "tp", None),
    )
    out_specs = (P("sp", "tp"), P("tp", None, None), P("sp", "tp", None))
    return jax.shard_map(
        on_device, mesh=mesh, in_specs=in_specs, out_specs=out_specs, check_vma=False
    )
```

time: 73.1 us -> 62.5 us (0.85)
  the two profiles are of different devices: /device:TPU:64 before, /device:TPU:24 now
where the time goes in v2:
time: 62.5 us; the launch traced here: 62.3 us
  Pallas kernels  58.9 us (94%)
  local copies, waits for them, and re-layouts  2.68 us (4%)
  between operations  0.65 us (1%)
    pallas_call x1, Pallas kernels, fused(): pl.pallas_call(kernel, out_shape=(jax.ShapeDtypeStruct((rows, DK), BF16),...  58.9 us
    unnamed x7, local copies, waits for them, and re-layouts  2.68 us

profile of v2, /device:TPU:24, one launch (start us, length us, event | category | flops | bytes accessed | tf_op | source)
XLA Modules:
  0.0 62.3 jit_solution(1381913445583054498)
XLA Ops:
  0.6 58.9 %shard_map.130 = (bf16[384,128]{1,0:T(8,128)(2,1)}, bf16[1,128,128]{2,1,0:T(8,128)(2,1)}, f32[1,1,128]{2,1,0:T(1,128)}) custom-call(bf16[384,256]{1,0:T(8,128)(2,1)} %x_hbm.1, bf16[2048,128]{1,0:T(8,128)(2,1)} %wq_hbm.1, bf16[2048,128]{1,0:T(8,128)(2,1)} %wk_hbm.1, bf16[2048,128]{1,0:T(8,128)(2,1)} %wv_hbm.1, bf16[2048,128]{1,0:T(8,128)(2,1)} %wz_hbm.1, ...), custom_call_target="tpu_custom_call" | custom-call | tf_op jit(solution)/shard_map/pallas_call | solution.py:420
  59.6 0.0 copy-start
  59.6 1.5 %copy.17 = bf16[384,128]{1,0:T(8,128)(2,1)} copy(bf16[384,128]{1,0:T(8,128)(2,1)} %get-tuple-element.6) | data formatting | bytes 196608
  61.1 0.0 copy-done
  61.1 0.0 copy-start.1
  61.1 0.6 copy.18
  61.7 0.0 copy-done.1
  61.7 0.5 copy.19
Async XLA Ops:
  59.6 1.6 %copy-start = (bf16[1,128,128]{2,1,0:T(8,128)(2,1)S(1)}, bf16[1,128,128]{2,1,0:T(8,128)(2,1)}, u32[]{:S(2)}) copy-start(bf16[1,128,128]{2,1,0:T(8,128)(2,1)} %get-tuple-element.7) | copy-start | bytes 98308
  61.1 0.6 %copy-start.1 = (f32[1,1,128]{2,1,0:T(1,128)S(1)}, f32[1,1,128]{2,1,0:T(1,128)}, u32[]{:S(2)}) copy-start(f32[1,1,128]{2,1,0:T(1,128)} %get-tuple-element.8) | copy-start | bytes 1540

commit v3 on v2

--- a/solution.py
+++ b/solution.py
@@ -65,16 +65,19 @@
     t, y4 = t + dot3(t, y2, BNN), dot3(y2, y2, BNN)
     t = t + dot3(t, y4, BNN)
     while size < ROWS:
-        joins = (row // (2 * size) == col // (2 * size)) & (row // size != col // size)
-        t = t - dot2(t, dot2(jnp.where(joins, a, 0.0), t, BNN), BNN)
-        size *= 2
+        joins = (row // (4 * size) == col // (4 * size)) & (row // size != col // size)
+        n = dot2(t, jnp.where(joins, a, 0.0), BNN)
+        t, n2 = t - dot2(n, t, BNN), dot2(n, n, BNN)
+        t = t + dot2(n2, t, BNN)
+        size *= 4
     return t
 
 
 def kernel(
     x_hbm, wq_hbm, wk_hbm, wv_hbm, wz_hbm, wr_hbm,
+    taps_hbm, speed_hbm, logs_hbm, gain_hbm, probe_hbm,
+    mixed_ref, cache_ref, read_ref,
     taps_ref, speed_ref, logs_ref, gain_ref, probe_ref,
-    mixed_ref, cache_ref, read_ref,
     x_all, x_tail, w_all, w_rate, tail, rim_in, ext, gates,
     q_ref, k_ref, kb_ref, vb_ref, a_ref, sum_ref, decay_ref,
     board_0, board_1, board_2,
@@ -101,27 +104,15 @@
         digit = digits[level]
         return sp + ((digit + turn) % counts[level] - digit) * strides[level]
 
-    def columns(slot):
-        return pl.ds(pl.multiple_of(slot * width, width), width)
-
     def near(r):
         return ((chip + r) % 4) * 2 + core
 
-    load_x = pltpu.make_async_copy(x_hbm, x_all.at[:, columns(tp)], load_sem.at[0])
+    load_x = pltpu.make_async_copy(x_hbm, x_all.at[tp], load_sem.at[0])
     load_x.start()
     load_tail = pltpu.make_async_copy(
-        x_hbm.at[pl.ds(rows - RIM, RIM), :], x_tail.at[:, columns(tp)], load_sem.at[6]
+        x_hbm.at[pl.ds(rows - RIM, RIM), :], x_tail.at[tp], load_sem.at[6]
     )
     load_tail.start()
-    loads = []
-    for i, w in enumerate((wq_hbm, wk_hbm, wv_hbm, wz_hbm)):
-        loads.append(
-            pltpu.make_async_copy(w, w_all.at[:, pl.ds(i * DK, DK)], load_sem.at[1 + i])
-        )
-    loads.append(pltpu.make_async_copy(wr_hbm, w_rate, load_sem.at[5]))
-    for load in loads:
-        load.start()
-
     after, before_sp = (sp + 1) % n_sp, (sp + n_sp - 1) % n_sp
     barrier = pltpu.get_barrier_semaphore()
     greeted = [(sp, near(r)) for r in (2, 1, 3)] + [(sp, partner), (after, tp), (before_sp, tp)]
@@ -130,6 +121,21 @@
     greeted += [(member(2, turn), tp) for turn in beyond]
     for peer in greeted:
         pl.semaphore_signal(barrier, inc=1, device_id=peer, device_id_type=MESH)
+    loads = []
+    for i, w in enumerate((wq_hbm, wk_hbm, wv_hbm, wz_hbm)):
+        loads.append(
+            pltpu.make_async_copy(w, w_all.at[i], load_sem.at[1 + i])
+        )
+    loads.append(pltpu.make_async_copy(wr_hbm, w_rate, load_sem.at[5]))
+    small = (
+        (taps_hbm, taps_ref), (speed_hbm, speed_ref), (logs_hbm, logs_ref),
+        (gain_hbm, gain_ref), (probe_hbm, probe_ref),
+    )
+    for i, (source, place) in enumerate(small):
+        loads.append(pltpu.make_async_copy(source, place, load_sem.at[7 + i]))
+    for load in loads:
+        load.start()
+
     load_x.wait()
     load_tail.wait()
     pl.semaphore_wait(barrier, len(greeted))
@@ -145,8 +151,8 @@
 
     def block(part, slot):
         if part == parts:
-            return x_tail.at[:, columns(slot)]
-        return x_all.at[pl.ds(part * ROWS, ROWS), columns(slot)]
+            return x_tail.at[slot]
+        return x_all.at[slot, pl.ds(part * ROWS, ROWS)]
 
     def to(place, peer, send, recv):
         copy = pltpu.make_async_remote_copy(
@@ -184,7 +190,10 @@
         passes.extend(mine)
 
     gathered(parts)
-    tail[...] = dot(x_tail[...], w_all[:, pl.ds(0, 3 * DK)], NN).astype(BF16)
+    slots = x_all.shape[0]
+    tail_x = jnp.concatenate([x_tail[slot] for slot in range(slots)], axis=1)
+    three = jnp.concatenate([w_all[i] for i in range(3)], axis=1)
+    tail[...] = dot(tail_x, three, NN).astype(BF16)
     rim_copy = pltpu.make_async_remote_copy(
         src_ref=tail, dst_ref=rim_in, send_sem=rim_sem.at[0], recv_sem=rim_sem.at[1],
         device_id=(after, tp), device_id_type=MESH,
@@ -197,11 +206,14 @@
     eye = (row == col).astype(F32)
     below = (row >= col).astype(BF16)
     gain_row = gain_ref[...].astype(F32)
+    own_head = lax.broadcasted_iota(jnp.int32, speed_ref.shape, 1) == tp
+    speed = jnp.sum(jnp.where(own_head, speed_ref[...], 0.0), axis=-1, keepdims=True)
 
     def prepare(part):
         here = pl.ds(part * ROWS, ROWS)
-        x = x_all[here, :]
-        raw = dot(x, w_all[...], NN).astype(BF16).astype(F32)
+        x = jnp.concatenate([x_all[slot, here, :] for slot in range(slots)], axis=1)
+        four = jnp.concatenate([w_all[i] for i in range(4)], axis=1)
+        raw = dot(x, four, NN).astype(BF16).astype(F32)
         rates = dot(x, w_rate[...], NT)
         ext[pl.ds(RIM + part * ROWS, ROWS), :] = raw[:, : 3 * DK]
         gates[here, :] = silu(raw[:, 3 * DK :]) * gain_row
@@ -226,7 +238,7 @@
         write = jnp.sum(jnp.where(kind == tp + kinds // 2, rates, 0.0), axis=-1, keepdims=True)
         beta = jax.nn.sigmoid(write - math.log(4.0 * rows * n_sp / DK))
         soft = jnp.maximum(fade, 0.0) + jnp.log1p(jnp.exp(-jnp.abs(fade)))
-        spread = jnp.broadcast_to(logs_ref[:, here], (ROWS, ROWS)).T - speed_ref[tp] * soft
+        spread = jnp.broadcast_to(logs_ref[:, here], (ROWS, ROWS)).T - speed * soft
         high, low = halves(spread)
         lowest = (spread - high.astype(F32) - low.astype(F32)).astype(BF16)
         summed = dot(below, high, NN) + (dot(below, low, NN) + dot(below, lowest, NN))
@@ -254,24 +266,22 @@
     t_mat = inverse_of_unit_lower(a_ref[...], row[None], col[None])
     grown = jnp.exp(summed)
     right = jnp.concatenate([k_beta * grown, vb_ref[...]], axis=2)
-    wu = dot3(t_mat, right, BNN)
+    wu = dot2(t_mat, right, BNN)
     k_dec = keys * jnp.exp(summed[:, ROWS - 1 :, :] - summed)
     last = grown[:, ROWS - 1 :, :]
 
-    news, starts, gains = [], [], []
-    m = None
-    gain = jnp.ones((1, DK), F32)
+    starts, gains = [], []
+    m, gain = None, jnp.ones((1, DK), F32)
     for part in range(parts):
-        w = wu[part, :, :DK]
-        new = jnp.concatenate([gain * w, wu[part, :, DK:]], axis=1)
-        if m is not None:
-            new = new - dot3(w, m, NN)
-        news.append(new)
+        step = dot3(k_dec[part], wu[part], TN)
         starts.append(m)
         gains.append(gain)
-        step = dot3(k_dec[part], new, TN)
-        twice = jnp.concatenate([last[part], last[part]], axis=1)
-        m = step if m is None else twice * m + step
+        if m is None:
+            m = step
+        else:
+            twice = jnp.concatenate([last[part], last[part]], axis=1)
+            scaled = jnp.concatenate([gain * step[:, :DK], step[:, DK:]], axis=1)
+            m = twice * m - dot2(step[:, :DK], m, NN) + scaled
         gain = gain * last[part]
 
     def gain_rows(gain):
@@ -350,9 +360,13 @@
     attend = dot3(query, keys, BNT) * decay
     q_dec = query * grown
     for part in range(parts):
-        both = dot3(attend[part], news[part], NN)
+        w = wu[part, :, :DK]
+        new = jnp.concatenate([gains[part] * w, wu[part, :, DK:]], axis=1)
         if starts[part] is not None:
-            both = both + dot3(q_dec[part], starts[part], NN)
+            new = new - dot2(w, starts[part], NN)
+        both = dot2(attend[part], new, NN)
+        if starts[part] is not None:
+            both = both + dot2(q_dec[part], starts[part], NN)
         coupling.append(gains[part] * q_dec[part] - both[:, :DK])
         base.append(both[:, DK:])
     coupling = jnp.concatenate(coupling, axis=0)
@@ -369,7 +383,7 @@
         else:
             quarters = post_quarters(m, gain)
             sent += list(quarters.values())
-        both = dot3(coupling, before, NN)
+        both = dot2(coupling, before, NN)
         coupling = before_gain * coupling - both[:, :DK]
         base = base + both[:, DK:]
     passed = []
@@ -384,17 +398,41 @@
         copy.wait_recv()
     sent += passed
 
-    def part_of(i, lanes):
-        return board_2[i, :, pl.ds(0, SHARE), lanes].reshape(DK, DK)
-
-    state = part_of(0, pl.ds(DK, DK)).astype(F32)
+    def group(i):
+        whole = board_2[i, :, pl.ds(0, SHARE), :].astype(F32).reshape(DK, 2 * DK)
+        return whole, gain_of(board_2[i, 0, pl.ds(SHARE, EXTRA), :])
+
+    def then(first, second):
+        (m, gain), (m2, gain2) = first, second
+        scaled = jnp.concatenate([gain[:, :DK] * m2[:, :DK], m2[:, DK:]], axis=1)
+        return gain2 * m - dot2(m2[:, :DK], m, NN) + scaled, gain * gain2
+
+    def step(state, element):
+        m, gain = element
+        return gain[:, :DK] * state - dot2(m[:, :DK], state, NN) + m[:, DK:]
+
+    runs = {1: [group(i) for i in range(far)]}
+    size = 1
+    while 2 * size < far:
+        runs[2 * size] = [
+            then(runs[size][j], runs[size][j + 1]) if j else None
+            for j in range(0, len(runs[size]), 2)
+        ]
+        size *= 2
+    states = {1: runs[1][0][0][:, DK:]}
+    size = 1
+    while size < far:
+        states[2 * size] = step(states[size], runs[size][1])
+        size *= 2
+    while size > 1:
+        size //= 2
+        for at in range(2 * size, far, 2 * size):
+            states[at + size] = step(states[at], runs[size][at // size])
+    state = states[far]
     entry = jnp.zeros((DK, DK), F32)
     for i in range(1, far):
-        entry = jnp.where(digits[2] == i, state, entry)
-        g2 = gain_of(board_2[i, 0, pl.ds(SHARE, EXTRA), pl.ds(0, DK)])
-        added = part_of(i, pl.ds(DK, DK)).astype(F32)
-        state = apply(part_of(i, pl.ds(0, DK)), g2, state) + added
-    out = base + dot3(coupling, entry, NN)
+        entry = jnp.where(digits[2] == i, states[i], entry)
+    out = base + dot2(coupling, entry, NN)
     normed = out * lax.rsqrt(jnp.mean(out * out, axis=-1, keepdims=True) + EPS)
     mixed_ref[...] = (normed * gates[...]).astype(BF16)
     cache = state.astype(BF16)
@@ -411,10 +449,10 @@
 def fused(x, wq, wk, wv, wz, wr, taps, speed, logs, gain, probe):
     rows = x.shape[0]
     depth = wq.shape[0]
+    slots = depth // x.shape[1]
     parts = rows // ROWS
     any_space = pl.BlockSpec(memory_space=pl.ANY)
     vmem = pl.BlockSpec(memory_space=pltpu.VMEM)
-    smem = pl.BlockSpec(memory_space=pltpu.SMEM)
     dma = pltpu.SemaphoreType.DMA
     block = pltpu.VMEM((parts, ROWS, DK), F32)
     return pl.pallas_call(
@@ -424,12 +462,13 @@
             jax.ShapeDtypeStruct((1, DK, DK), BF16),
             jax.ShapeDtypeStruct((1, 1, DK), F32),
         ),
-        in_specs=[any_space] * 6 + [vmem, smem, vmem, vmem, vmem],
+        in_specs=[any_space] * 11,
         out_specs=(vmem, vmem, vmem),
         scratch_shapes=[
-            pltpu.VMEM((rows, depth), BF16),
-            pltpu.VMEM((RIM, depth), BF16),
-            pltpu.VMEM((depth, 4 * DK), BF16),
+            *[pltpu.VMEM(a.shape, a.dtype) for a in (taps, speed, logs, gain, probe)],
+            pltpu.VMEM((slots, rows, depth // slots), BF16),
+            pltpu.VMEM((slots, RIM, depth // slots), BF16),
+            pltpu.VMEM((4, depth, DK), BF16),
             pltpu.VMEM(wr.shape, BF16),
             pltpu.VMEM((RIM, 3 * DK), BF16),
             pltpu.VMEM((RIM, 3 * DK), BF16),
@@ -439,7 +478,7 @@
             pltpu.VMEM((4, DK + EXTRA, 2 * DK), BF16),
             pltpu.VMEM((2, DK + EXTRA, 2 * DK), BF16),
             pltpu.VMEM((8, 4, SHARE + EXTRA, 2 * DK), BF16),
-            dma((7,)),
+            dma((12,)),
             dma((parts + 1, 4)),
             dma((parts + 1, 4)),
             dma((parts + 1, 4)),
@@ -458,7 +497,7 @@
 def on_device(x, wq, wk, wv, wz, wr, taps, speed, logs, gain, probe):
     by_kind = wr.transpose(0, 2, 1).reshape(-1, wr.shape[1])
     return fused(
-        x, wq, wk, wv, wz, by_kind, taps, speed, logs.reshape(1, -1), gain.reshape(1, DK), probe
+        x, wq, wk, wv, wz, by_kind, taps, speed.reshape(1, -1), logs.reshape(1, -1), gain.reshape(1, DK), probe
     )
 
 

time: 62.5 us -> 60.2 us (0.963)
  Pallas kernels: 58.9 us -> 56.7 us
    pallas_call x1, Pallas kernels: 58.9 us -> 56.7 us  [fused(): pl.pallas_call(kernel, out_shape=(jax.ShapeDtypeStruct((rows, DK), BF16),...]
where the time goes in v3:
time: 60.2 us; the launch traced here: 60 us
  Pallas kernels  56.7 us (94%)
  local copies, waits for them, and re-layouts  2.68 us (4%)
  between operations  0.65 us (1%)
    pallas_call x1, Pallas kernels, fused(): pl.pallas_call(kernel, out_shape=(jax.ShapeDtypeStruct((rows, DK), BF16),...  56.7 us
    unnamed x7, local copies, waits for them, and re-layouts  2.68 us

profile of v3, /device:TPU:24, one launch (start us, length us, event | category | flops | bytes accessed | tf_op | source)
XLA Modules:
  0.0 60.0 jit_solution(6500293966675005683)
XLA Ops:
  0.6 56.7 %shard_map.130 = (bf16[384,128]{1,0:T(8,128)(2,1)}, bf16[1,128,128]{2,1,0:T(8,128)(2,1)}, f32[1,1,128]{2,1,0:T(1,128)}) custom-call(bf16[384,256]{1,0:T(8,128)(2,1)} %x_hbm.1, bf16[2048,128]{1,0:T(8,128)(2,1)} %wq_hbm.1, bf16[2048,128]{1,0:T(8,128)(2,1)} %wk_hbm.1, bf16[2048,128]{1,0:T(8,128)(2,1)} %wv_hbm.1, bf16[2048,128]{1,0:T(8,128)(2,1)} %wz_hbm.1, ...), custom_call_target="tpu_custom_call" | custom-call | tf_op jit(solution)/shard_map/pallas_call | solution.py:458
  57.3 0.0 copy-start
  57.3 1.5 %copy.17 = bf16[384,128]{1,0:T(8,128)(2,1)} copy(bf16[384,128]{1,0:T(8,128)(2,1)} %get-tuple-element.6) | data formatting | bytes 196608
  58.9 0.0 copy-done
  58.9 0.0 copy-start.1
  58.9 0.6 %copy.18 = bf16[1,128,128]{2,1,0:T(8,128)(2,1)} copy(bf16[1,128,128]{2,1,0:T(8,128)(2,1)S(1)} %copy-done) | data formatting | bytes 65536
  59.5 0.0 copy-done.1
  59.5 0.5 copy.19
Async XLA Ops:
  57.3 1.6 %copy-start = (bf16[1,128,128]{2,1,0:T(8,128)(2,1)S(1)}, bf16[1,128,128]{2,1,0:T(8,128)(2,1)}, u32[]{:S(2)}) copy-start(bf16[1,128,128]{2,1,0:T(8,128)(2,1)} %get-tuple-element.7) | copy-start | bytes 98308
  58.9 0.6 %copy-start.1 = (f32[1,1,128]{2,1,0:T(1,128)S(1)}, f32[1,1,128]{2,1,0:T(1,128)}, u32[]{:S(2)}) copy-start(f32[1,1,128]{2,1,0:T(1,128)} %get-tuple-element.8) | copy-start | bytes 1540

commit v4 on v3

--- a/solution.py
+++ b/solution.py
@@ -332,27 +332,19 @@
 
     def read(level, i):
         board = boards[level]
-        transition = board[i, pl.ds(0, DK), pl.ds(0, DK)]
-        whole = board[i, pl.ds(0, DK), :].astype(F32)
-        return transition, whole, gain_of(board[i, pl.ds(DK, EXTRA), :])
-
-    def apply(transition, g2, m):
-        high, low = halves(m)
-        wide = jnp.concatenate([transition, transition], axis=1)
-        return g2 * m - dot(wide, jnp.concatenate([high, low], axis=0), NN)
-
-    def compose(level):
-        digit = digits[level]
-        _, m, gain = read(level, 0)
-        before, before_gain = jnp.zeros((DK, 2 * DK), F32), jnp.ones((1, 2 * DK), F32)
-        for i in range(1, counts[level]):
-            before = jnp.where(digit == i, m, before)
-            before_gain = jnp.where(digit == i, gain, before_gain)
-            transition, own_m, g2 = read(level, i)
-            scaled = jnp.concatenate([gain[:, :DK] * own_m[:, :DK], own_m[:, DK:]], axis=1)
-            m = apply(transition, g2, m) + scaled
-            gain = gain * g2
-        return m, gain[:, :DK], before, before_gain[:, :DK]
+        return board[i, pl.ds(0, DK), :].astype(F32), gain_of(board[i, pl.ds(DK, EXTRA), :])
+
+    def then(first, second):
+        (m, gain), (m2, gain2) = first, second
+        scaled = jnp.concatenate([gain[:, :DK] * m2[:, :DK], m2[:, DK:]], axis=1)
+        return gain2 * m - dot2(m2[:, :DK], m, NN) + scaled, gain * gain2
+
+    def choose(level, before):
+        m, gain = jnp.zeros((DK, 2 * DK), F32), jnp.ones((1, 2 * DK), F32)
+        for i, (m_i, gain_i) in enumerate(before):
+            m = jnp.where(digits[level] == i + 1, m_i, m)
+            gain = jnp.where(digits[level] == i + 1, gain_i, gain)
+        return m, gain[:, :DK]
 
     copies = post(0, m, gain)
 
@@ -376,20 +368,26 @@
     for level in range(2):
         for copy in copies:
             copy.wait_recv()
-        m, gain, before, before_gain = compose(level)
+        members = [read(level, i) for i in range(counts[level])]
+        left = then(members[0], members[1])
         if level == 0:
-            copies = post(1, m, gain)
+            m, gain = then(left, then(members[2], members[3]))
+            copies = post(1, m, gain[:, :DK])
             sent += copies
+            known = [members[0], left, then(left, members[2])]
         else:
-            quarters = post_quarters(m, gain)
+            m, gain = left
+            quarters = post_quarters(m, gain[:, :DK])
             sent += list(quarters.values())
+            known = [members[0]]
+        before, before_gain = choose(level, known)
         both = dot2(coupling, before, NN)
         coupling = before_gain * coupling - both[:, :DK]
         base = base + both[:, DK:]
     passed = []
     for turn in turns[2]:
         quarters[turn].wait_recv()
-        place = board_2.at[(digits[2] + far - turn) % far, digits[0]]
+        place = board_2.at[(digits[2] + far - turn) % far, digits[0], pl.ds(0, SHARE), :]
         for side in turns[0]:
             passed.append(
                 remote(place, 0, side, pass_sem.at[turn, side], got_sem.at[turn, side])
@@ -400,12 +398,7 @@
 
     def group(i):
         whole = board_2[i, :, pl.ds(0, SHARE), :].astype(F32).reshape(DK, 2 * DK)
-        return whole, gain_of(board_2[i, 0, pl.ds(SHARE, EXTRA), :])
-
-    def then(first, second):
-        (m, gain), (m2, gain2) = first, second
-        scaled = jnp.concatenate([gain[:, :DK] * m2[:, :DK], m2[:, DK:]], axis=1)
-        return gain2 * m - dot2(m2[:, :DK], m, NN) + scaled, gain * gain2
+        return whole, gain_of(board_2[i, digits[0], pl.ds(SHARE, EXTRA), :])
 
     def step(state, element):
         m, gain = element
@@ -494,11 +487,28 @@
     )(x, wq, wk, wv, wz, wr, taps, speed, logs, gain, probe)
 
 
+def placed_kernel(mixed, cache, read, mixed_out, cache_out, read_out):
+    mixed_out[...] = mixed[...]
+    cache_out[...] = cache[...]
+    read_out[...] = read[...]
+
+
+def placed(outs):
+    vmem = pl.BlockSpec(memory_space=pltpu.VMEM)
+    return pl.pallas_call(
+        placed_kernel,
+        out_shape=tuple(jax.ShapeDtypeStruct(out.shape, out.dtype) for out in outs),
+        in_specs=[vmem] * 3,
+        out_specs=(vmem,) * 3,
+    )(*outs)
+
+
 def on_device(x, wq, wk, wv, wz, wr, taps, speed, logs, gain, probe):
     by_kind = wr.transpose(0, 2, 1).reshape(-1, wr.shape[1])
-    return fused(
+    outs = fused(
         x, wq, wk, wv, wz, by_kind, taps, speed.reshape(1, -1), logs.reshape(1, -1), gain.reshape(1, DK), probe
     )
+    return placed(outs)
 
 
 def solution(mesh):

time: 60.2 us -> 59 us (0.980)
  local copies, waits for them, and re-layouts: 2.68 us -> 0 us
  Pallas kernels: 56.7 us -> 58.2 us
    unnamed x7 -> x0, local copies, waits for them, and re-layouts: 2.68 us -> none
    pallas_call x0 -> x1, Pallas kernels: none -> 1.57 us  [placed(): pl.pallas_call(placed_kernel, out_shape=tuple((jax.ShapeDtypeStruct(out.s...]
where the time goes in v4:
time: 59 us; the launch traced here: 58.8 us
  Pallas kernels  58.2 us (99%)
  between operations  0.64 us (1%)
    pallas_call x1, Pallas kernels, fused(): pl.pallas_call(kernel, out_shape=(jax.ShapeDtypeStruct((rows, DK), BF16),...  56.6 us
    pallas_call x1, Pallas kernels, placed(): pl.pallas_call(placed_kernel, out_shape=tuple((jax.ShapeDtypeStruct(out.s...  1.57 us

profile of v4, /device:TPU:24, one launch (start us, length us, event | category | flops | bytes accessed | tf_op | source)
XLA Modules:
  0.0 58.8 jit_solution(4566621188865578485)
XLA Ops:
  0.6 56.6 %shard_map.130 = (bf16[384,128]{1,0:T(8,128)(2,1)}, bf16[1,128,128]{2,1,0:T(8,128)(2,1)}, f32[1,1,128]{2,1,0:T(1,128)}) custom-call(bf16[384,256]{1,0:T(8,128)(2,1)} %x_hbm.1, bf16[2048,128]{1,0:T(8,128)(2,1)} %wq_hbm.1, bf16[2048,128]{1,0:T(8,128)(2,1)} %wk_hbm.1, bf16[2048,128]{1,0:T(8,128)(2,1)} %wv_hbm.1, bf16[2048,128]{1,0:T(8,128)(2,1)} %wz_hbm.1, ...), custom_call_target="tpu_custom_call" | custom-call | tf_op jit(solution)/shard_map/pallas_call | solution.py:451
  57.3 1.6 %shard_map.131 = (bf16[384,128]{1,0:T(8,128)(2,1)}, bf16[1,128,128]{2,1,0:T(8,128)(2,1)}, f32[1,1,128]{2,1,0:T(1,128)}) custom-call(bf16[384,128]{1,0:T(8,128)(2,1)} %get-tuple-element.6.mixed, bf16[1,128,128]{2,1,0:T(8,128)(2,1)} %get-tuple-element.7.cache, f32[1,1,128]{2,1,0:T(1,128)} %get-tuple-element.8.read), custom_call_target="tpu_custom_call" | custom-call | tf_op jit(solution)/shard_map/pallas_call | solution.py:498
